TPU v7x, 32 devices: a whole 2x2x4 slice. The times are simulated.
32 devices in a mesh: sp: 8 (over z, x), tp: 4 (over y, core).
Axes of the slice: x: 2, y: 2, z: 4, core: 2. Of those that a mesh axis runs over, the one named last changes fastest.
Arguments:
- query_logits: bfloat16 [4096, 4096], P('sp', 'tp'), may hold values from -6 to 6
- forget_logits: bfloat16 [4096, 4096], P('sp', 'tp'), may hold values from -6 to 6
- value_inputs: bfloat16 [4096, 4096], P('sp', 'tp'), may hold values from -16 to 16
- output_gate_logits: bfloat16 [4096, 4096], P('sp', 'tp'), may hold values from -6 to 6
- forget_floor_gap: float32 [4096], replicated, may hold values from 2.4414063e-05 to 0.1
- surge_log_decay: float32 [32, 4096], P('tp', 'sp'), may hold values from -0.7 to 0
- head_norm_gain: float32 [128], replicated, may hold values from 0.1 to 1.9
- output_matrix: bfloat16 [4096, 4096], P('sp', 'tp'), may hold values from -1.25 to 1.25
- branch_norm_gain: float32 [4096], replicated, may hold values from 0.1 to 1.9
- residual: bfloat16 [4096, 4096], P('sp', 'tp'), may hold values from -6 to 6
Outputs:
- output: bfloat16 [4096, 4096], P('sp', 'tp')
All inputs are finite; a program needn't handle non-finite values.
Results may differ from a plain program's by a relative error of at most 0.005.
Values may be sent and summed in bfloat16 or wider, within the bound.
A program may use at most 128 MiB of HBM per device.

v0:
```python
import functools

import jax
import jax.numpy as jnp
from jax import lax
from jax.experimental import pallas as pl
from jax.experimental.pallas import tpu as pltpu
from jax.sharding import Mesh
from jax.sharding import PartitionSpec as P

HEAD_DIM = 128
SPAN = 128
TAIL = 16
EPSILON = 1e-06
NT = (((1,), (1,)), ((), ()))
TN = (((0,), (0,)), ((), ()))
NN = (((1,), (0,)), ((), ()))
MESH_ID = pl.DeviceIdType.MESH


def dot(a, b, dims=NN):
    return lax.dot_general(a, b, dims, preferred_element_type=jnp.float32)


def lower_triangle():
    rows = lax.broadcasted_iota(jnp.int32, (SPAN, SPAN), 0)
    columns = lax.broadcasted_iota(jnp.int32, (SPAN, SPAN), 1)
    return rows >= columns


def diagonal():
    rows = lax.broadcasted_iota(jnp.int32, (SPAN, SPAN), 0)
    columns = lax.broadcasted_iota(jnp.int32, (SPAN, SPAN), 1)
    return rows == columns


def silu(logits):
    return logits / (1.0 + jnp.exp(-logits))


def decays(logits, gap, surge, causal):
    keys = gap / (1.0 + jnp.exp(logits.astype(jnp.float32)))
    series = keys * (1.0 / 7.0) + (1.0 / 6.0)
    for order in (5, 4, 3, 2):
        series = series * keys + (1.0 / order)
    logs = -(series * keys + 1.0) * keys
    high = logs.astype(jnp.bfloat16)
    low = (logs - high.astype(jnp.float32)).astype(jnp.bfloat16)
    ones = causal.astype(jnp.bfloat16)
    surged = jnp.sum(jnp.where(causal, surge, 0.0), axis=1, keepdims=True)
    return keys, dot(ones, high) + dot(ones, low) + surged


def layer_kernel(
    sizes,
    query_in,
    forget_in,
    value_in,
    gate_in,
    gap_ref,
    surge_ref,
    gain_ref,
    weight_in,
    projected_ref,
    scale_ref,
    whole_weight,
    query_ref,
    forget_ref,
    value_ref,
    gate_ref,
    running_ref,
    keys_ref,
    base_ref,
    starts_ref,
    state_out,
    gathered,
    chain_in,
    chain_out,
    deliver_out,
    carried,
    local_ref,
    reach_ref,
    gated_ref,
    mixed_ref,
    partial_out,
    partial_in,
    total_ref,
    sums_ref,
    squares_ref,
    load_sems,
    gather_send,
    gather_recv,
    chain_send,
    chain_recv,
    deliver_send,
    deliver_recv,
    swap_send,
    swap_recv,
    tp_send,
    tp_recv,
    line_send,
    line_recv,
    side_sems,
    partial_send,
    partial_recv,
    square_send,
    square_recv,
):
    hi_size, inner_size, tp_size, per, tile, weight_tile = sizes
    rows, width = query_in.shape
    depth, columns = weight_in.shape
    heads = width // HEAD_DIM
    spans = rows // SPAN
    groups = heads // per
    half_width = heads * tp_size // 2 * HEAD_DIM
    members = 2 * inner_size
    own_heads = heads // members
    tiles = columns // tile
    pieces = columns // weight_tile
    near = hi_size // 2 * per * HEAD_DIM
    away = half_width - near
    hi, lo, inner, tp = (lax.axis_index(a) for a in ("hi", "lo", "inner", "tp"))
    member = lo * inner_size + inner
    strides = []
    by = tp_size // 2
    while by >= 1:
        strides.append(by)
        by //= 2

    def member_at(index):
        return {"lo": index // inner_size, "inner": index % inner_size}

    def flipped(index, by):
        return index + by - 2 * by * ((index // by) % 2)

    def remote(source, target, send, recv, device):
        return pltpu.make_async_remote_copy(
            src_ref=source,
            dst_ref=target,
            send_sem=send,
            recv_sem=recv,
            device_id=device,
            device_id_type=MESH_ID,
        )

    def span_rows(span):
        return pl.ds(span * SPAN, SPAN)

    def lanes_of(head):
        return pl.ds(pl.multiple_of(head * HEAD_DIM, HEAD_DIM), HEAD_DIM)

    def slot_rows(block_hi, block_inner):
        return pl.ds(pl.multiple_of((block_hi * inner_size + block_inner) * depth, depth), depth)

    loads = [
        pltpu.make_async_copy(source, target, load_sems.at[number])
        for number, (source, target) in enumerate(
            (
                (weight_in, whole_weight.at[slot_rows(hi, inner)]),
                (forget_in, forget_ref),
                (value_in, value_ref),
                (query_in, query_ref),
                (gate_in, gate_ref),
            )
        )
    ]
    for load in loads:
        load.start()

    barrier = pltpu.get_barrier_semaphore()

    peers = members - 1 + tp_size - 1
    for step in range(1, members):
        pl.semaphore_signal(
            barrier,
            inc=1,
            device_id=member_at((member + step) % members),
            device_id_type=MESH_ID,
        )
    for step in range(1, tp_size):
        pl.semaphore_signal(
            barrier, inc=1, device_id={"tp": (tp + step) % tp_size}, device_id_type=MESH_ID
        )
    for step in (1, -1):
        there = hi + step
        inside = (there >= 0) & (there < hi_size)

        @pl.when(inside)
        def _():
            pl.semaphore_signal(barrier, inc=1, device_id={"hi": there}, device_id_type=MESH_ID)

        peers = peers + jnp.where(inside, 1, 0)
    pl.semaphore_wait(barrier, peers)

    def weight_block(block_hi, block_inner, piece):
        return whole_weight.at[
            slot_rows(block_hi, block_inner), pl.ds(piece * weight_tile, weight_tile)
        ]

    def step_of(way):
        return 1 if way == 0 else -1

    def line_copy(way, hop, piece):
        block = weight_block(hi - step_of(way) * (hop - 1), inner, piece)
        return remote(
            block,
            block,
            line_send.at[way, hop - 1],
            line_recv.at[hi - step_of(way) * (hop - 1), piece],
            {"hi": hi + step_of(way)},
        )

    def line_arrival(origin, piece):
        block = weight_block(origin, inner, piece)
        return remote(block, block, line_send.at[0, 0], line_recv.at[origin, piece], {"hi": origin})

    def line_sent(way, hop):
        block = whole_weight.at[slot_rows(0, 0)]
        return remote(
            block, block, line_send.at[way, hop - 1], line_recv.at[0, 0], {"hi": hi + step_of(way)}
        )

    def sends(way, hop):
        origin = hi - step_of(way) * (hop - 1)
        target = hi + step_of(way)
        return (origin >= 0) & (origin < hi_size) & (target >= 0) & (target < hi_size)

    def receives(way, hop):
        origin = hi - step_of(way) * hop
        return (origin >= 0) & (origin < hi_size)

    def side_copy(reach, block_hi, piece):
        block = weight_block(block_hi, inner, piece)
        return remote(
            block,
            block,
            side_sems.at[0, reach - 1, block_hi, piece],
            side_sems.at[1, reach - 1, block_hi, piece],
            {"inner": (inner + reach) % inner_size},
        )

    def start_line(way, piece):
        @pl.when(sends(way, 1))
        def _():
            line_copy(way, 1, piece).start()

    def start_side(piece):
        for reach in range(1, inner_size):
            side_copy(reach, hi, piece).start()

    def take_hop(hop, way, piece):
        if hop >= hi_size:
            return

        @pl.when(receives(way, hop))
        def _():
            line_arrival(hi - step_of(way) * hop, piece).wait_recv()
            for reach in range(1, inner_size):
                side_copy(reach, hi - step_of(way) * hop, piece).start()

        if hop + 1 < hi_size:

            @pl.when(sends(way, hop + 1))
            def _():
                line_copy(way, hop + 1, piece).start()

    near_first = hi < hi_size // 2
    near_block = jnp.where(near_first, 0, hi_size - hi_size // 2)
    away_block = jnp.where(near_first, hi_size // 2, 0)
    block_depth = per * HEAD_DIM

    def take_near_sides():
        for reach in range(1, inner_size):
            for number in range(hi_size // 2):
                for piece in range(pieces):
                    side_copy(reach, near_block + number, piece).wait_recv()

    def take_away_sides(piece):
        for reach in range(1, inner_size):
            for number in range(hi_size - hi_size // 2):
                side_copy(reach, away_block + number, piece).wait_recv()

    def state_copy(head):
        return remote(
            state_out.at[head],
            gathered.at[member, head % own_heads],
            gather_send.at[0],
            gather_recv.at[member, head % own_heads],
            member_at(head // own_heads),
        )

    def state_arrival(index, number):
        return remote(
            state_out.at[0],
            gathered.at[index, number],
            gather_send.at[0],
            gather_recv.at[index, number],
            member_at(index),
        )

    def chain_copy(number):
        return remote(
            chain_out.at[number],
            chain_in.at[number],
            chain_send.at[0],
            chain_recv.at[number],
            {"hi": hi + 1},
        )

    def deliver_copy(index, number):
        head = member * own_heads + number
        return remote(
            deliver_out.at[index * own_heads + number],
            carried.at[head],
            deliver_send.at[0],
            deliver_recv.at[head],
            member_at(index),
        )

    def deliver_arrival(head):
        return remote(
            deliver_out.at[0],
            carried.at[head],
            deliver_send.at[0],
            deliver_recv.at[head],
            member_at(head // own_heads),
        )

    def state_body(turn, carry):
        head = (turn + (member + 1) * own_heads) % heads
        causal = lower_triangle()
        gap = gap_ref[pl.ds(tp * heads + head, 1), :]
        lanes = lanes_of(head)
        this_head = lax.broadcasted_iota(jnp.int32, (heads, SPAN), 0) == head
        state = jnp.zeros((HEAD_DIM, HEAD_DIM), jnp.float32)
        base = jnp.zeros((1, HEAD_DIM), jnp.float32)
        for span in range(spans):
            part = span_rows(span)
            surge = jnp.sum(jnp.where(this_head, surge_ref[:, part], 0.0), axis=0, keepdims=True)
            keys, running = decays(forget_ref[part, lanes], gap, surge, causal)
            keys_ref[part, lanes] = keys
            running_ref[part, lanes] = running
            base_ref[head, span : span + 1, :] = base
            if span > 0:
                starts_ref[head, span - 1] = state.astype(jnp.bfloat16)
            ending = running[SPAN - 1 : SPAN, :]
            kept = (keys * jnp.exp(ending - running)).astype(jnp.bfloat16)
            state = state * jnp.exp(ending) + dot(value_ref[part, lanes], kept, TN)
            base = base + ending
        decay = jnp.exp(base)
        high = decay.astype(jnp.bfloat16).astype(jnp.float32)
        first = lax.broadcasted_iota(jnp.int32, (TAIL, HEAD_DIM), 0) == 0
        item = state.astype(jnp.bfloat16)
        tail = jnp.where(first, high, decay - high).astype(jnp.bfloat16)
        state_out[head, 0:HEAD_DIM, :] = item
        state_out[head, HEAD_DIM:, :] = tail
        owner = head // own_heads

        @pl.when(owner == member)
        def _():
            gathered[member, head % own_heads, 0:HEAD_DIM, :] = item
            gathered[member, head % own_heads, HEAD_DIM:, :] = tail

        @pl.when(owner != member)
        def _():
            state_copy(head).start()

        return carry

    def chain_states():
        @pl.when(hi == 0)
        def _():
            chain_in[...] = jnp.zeros_like(chain_in)

        def body(number, carry):
            for index in range(members):

                @pl.when(member != index)
                def _():
                    state_arrival(index, number).wait_recv()

            @pl.when(hi > 0)
            def _():
                chain_copy(number).wait_recv()

            state = chain_in[number].astype(jnp.float32)
            for index in range(members):
                deliver_out[index * own_heads + number] = state.astype(jnp.bfloat16)
                tail = gathered[index, number, HEAD_DIM:, :].astype(jnp.float32)
                item = gathered[index, number, 0:HEAD_DIM, :].astype(jnp.float32)
                state = state * (tail[0:1, :] + tail[1:2, :]) + item
            chain_out[number] = state.astype(jnp.bfloat16)

            @pl.when(hi + 1 < hi_size)
            def _():
                chain_copy(number).start()

            for index in range(members):

                @pl.when(member != index)
                def _():
                    deliver_copy(index, number).start()

            carried[member * own_heads + number] = deliver_out[member * own_heads + number]
            return carry

        lax.fori_loop(0, own_heads, body, 0)

    def take_states():
        def body(head, carry):
            @pl.when(head // own_heads != member)
            def _():
                deliver_arrival(head).wait_recv()

            return carry

        lax.fori_loop(0, heads, body, 0)

    gain = gain_ref[...]

    def local_body(head, carry):
        causal = lower_triangle()
        lanes = lanes_of(head)
        middle = SPAN // 2
        for span in range(spans):
            part = span_rows(span)
            running = running_ref[part, lanes]
            anchor = running[middle - 1 : middle, :]
            queries = silu(query_ref[part, lanes].astype(jnp.float32)) * (HEAD_DIM**-0.5)
            reach = queries * jnp.exp(running - anchor)
            back = keys_ref[part, lanes] * jnp.exp(anchor - running)
            scores = dot(reach.astype(jnp.bfloat16), back.astype(jnp.bfloat16), NT)
            scores = jnp.where(causal, scores, 0.0).astype(jnp.bfloat16)
            out = dot(scores, value_ref[part, lanes])
            if span > 0:
                out = out + dot(
                    (reach * jnp.exp(anchor)).astype(jnp.bfloat16), starts_ref[head, span - 1], NT
                )
            local_ref[part, lanes] = out
            base = base_ref[head, span : span + 1, :]
            reach_ref[part, lanes] = (reach * jnp.exp(anchor + base)).astype(jnp.bfloat16)
            gated_ref[part, lanes] = gain * silu(gate_ref[part, lanes].astype(jnp.float32))
        return carry

    def keeps(index, group):
        return (index * groups + group) % 2 == lo

    def group_lanes(index, group, which):
        start = which * half_width + (index * groups + group) // 2 * per * HEAD_DIM
        return pl.ds(pl.multiple_of(start, HEAD_DIM), per * HEAD_DIM)

    def swap_copy(group, span):
        start = 2 * half_width + group * per * HEAD_DIM
        return remote(
            mixed_ref.at[span_rows(span), pl.ds(start, per * HEAD_DIM)],
            mixed_ref.at[span_rows(span), group_lanes(tp, group, 1)],
            swap_send.at[group // 2],
            swap_recv.at[group // 2, span],
            {"lo": 1 - lo},
        )

    def origin_of(index, mask):
        for bit, by in enumerate(strides):
            if (mask >> bit) & 1:
                index = flipped(index, by)
        return index

    def tp_copy(stage, which, mask, group, span):
        block = mixed_ref.at[span_rows(span), group_lanes(origin_of(tp, mask), group, which)]
        return remote(
            block,
            block,
            tp_send.at[(1 << stage) - 1 + mask, which, group // 2],
            tp_recv.at[(1 << stage) - 1 + mask, which, group // 2, span],
            {"tp": flipped(tp, strides[stage])},
        )

    def mix(span):
        part = span_rows(span)
        for head in range(heads):
            lanes = lanes_of(head)
            out = local_ref[part, lanes] + dot(reach_ref[part, lanes], carried[head], NT)
            mean_sq = jnp.mean(out * out, axis=1, keepdims=True)
            mixed = out * lax.rsqrt(mean_sq + EPSILON) * gated_ref[part, lanes]
            group = head // per
            kept_start = (tp * groups + group) // 2 * per * HEAD_DIM + head % per * HEAD_DIM
            away_start = 2 * half_width + head * HEAD_DIM
            start = jnp.where(keeps(tp, group), kept_start, away_start)
            mixed_ref[part, pl.ds(pl.multiple_of(start, HEAD_DIM), HEAD_DIM)] = mixed.astype(
                jnp.bfloat16
            )

    def send_away(span):
        for group in range(groups):

            @pl.when(jnp.logical_not(keeps(tp, group)))
            def _():
                swap_copy(group, span).start()

    def send_kept(span):
        for group in range(groups):

            @pl.when(keeps(tp, group))
            def _():
                for stage in range(len(strides)):
                    tp_copy(stage, 0, 0, group, span).start()

    def take_swap(span):
        for group in range(groups):

            @pl.when(keeps(tp, group))
            def _():
                swap_copy(group, span).wait_recv()
                for stage in range(len(strides)):
                    tp_copy(stage, 1, 0, group, span).start()

    def take_stage(stage, which, span):
        peer = flipped(tp, strides[stage])
        for mask in range(1 << stage):
            for group in range(groups):

                @pl.when(keeps(origin_of(peer, mask), group))
                def _():
                    tp_copy(stage, which, mask, group, span).wait_recv()
                    for later in range(stage + 1, len(strides)):
                        tp_copy(later, which, mask | (1 << stage), group, span).start()

    def partial_copy(piece, span):
        return remote(
            partial_out.at[piece, span],
            partial_in.at[piece, span],
            partial_send.at[0],
            partial_recv.at[piece, span],
            {"lo": 1 - lo},
        )

    def both(span, start, depth):
        part = span_rows(span)
        start = pl.multiple_of(start, HEAD_DIM)
        later = pl.multiple_of(start + half_width, HEAD_DIM)
        return jnp.concatenate(
            [mixed_ref[part, pl.ds(later, depth)], mixed_ref[part, pl.ds(start, depth)]], axis=0
        )

    def multiply_near(span):
        start = near_block * block_depth
        left = both(span, start, near)
        rows_near = pl.ds(pl.multiple_of(start, HEAD_DIM), near)
        for number in range(tiles):
            lanes = pl.ds(number * tile, tile)
            total_ref[span, :, lanes] = dot(left, whole_weight[rows_near, lanes])

    def multiply_away(piece):
        start = away_block * block_depth
        rows_away = pl.ds(pl.multiple_of(start, HEAD_DIM), away)
        lanes = pl.ds(piece * weight_tile, weight_tile)
        right = whole_weight[rows_away, lanes]
        for span in range(spans):
            total = total_ref[span, :, lanes] + dot(both(span, start, away), right)
            partial_out[piece, span] = total[0:SPAN].astype(jnp.bfloat16)
            partial_copy(piece, span).start()
            total_ref[span, SPAN:, lanes] = total[SPAN:]

    def square_copy(step):
        return remote(
            squares_ref.at[tp],
            squares_ref.at[tp],
            square_send.at[step - 1],
            square_recv.at[step - 1],
            {"tp": (tp + step) % tp_size},
        )

    def combine(piece, span):
        lanes = pl.ds(piece * weight_tile, weight_tile)
        partial_copy(piece, span).wait_recv()
        total = total_ref[span, SPAN:, lanes] + partial_in[piece, span].astype(jnp.float32)
        rounded = total.astype(jnp.bfloat16)
        projected_ref[span_rows(span), lanes] = rounded
        branch = rounded.astype(jnp.float32)
        branch = branch * branch
        squares = branch[:, 0:HEAD_DIM]
        for start in range(HEAD_DIM, weight_tile, HEAD_DIM):
            squares = squares + branch[:, start : start + HEAD_DIM]
        if piece > 0:
            squares = squares + sums_ref[span]
        sums_ref[span] = squares

    def total_squares(span):
        column = jnp.sum(sums_ref[span], axis=1, keepdims=True)
        row = jnp.sum(jnp.where(diagonal(), column, 0.0), axis=0, keepdims=True)
        squares_ref[tp, span : span + 1, :] = row

    def finish():
        for step in range(1, tp_size):
            square_copy(step).wait_recv()
        total = squares_ref[0, 0:spans, :]
        for index in range(1, tp_size):
            total = total + squares_ref[index, 0:spans, :]
        scale_ref[...] = lax.rsqrt(total * (1.0 / (columns * tp_size)) + EPSILON)

    def lines_sent(first, last):
        for hop in range(first, last):
            for way in (0, 1):

                @pl.when(sends(way, hop))
                def _():
                    line_sent(way, hop).wait_send()

    def states_sent():
        others = (members - 1) * own_heads
        next_member = member_at((member + 1) % members)
        pltpu.make_async_remote_copy(
            src_ref=state_out.at[pl.ds(0, others)],
            dst_ref=state_out.at[pl.ds(0, others)],
            send_sem=gather_send.at[0],
            recv_sem=gather_recv.at[0, 0],
            device_id=next_member,
            device_id_type=MESH_ID,
        ).wait_send()
        pltpu.make_async_remote_copy(
            src_ref=deliver_out.at[pl.ds(0, others)],
            dst_ref=deliver_out.at[pl.ds(0, others)],
            send_sem=deliver_send.at[0],
            recv_sem=deliver_recv.at[0],
            device_id=next_member,
            device_id_type=MESH_ID,
        ).wait_send()

        @pl.when(hi + 1 < hi_size)
        def _():
            remote(
                chain_out, chain_in, chain_send.at[0], chain_recv.at[0], {"hi": hi + 1}
            ).wait_send()

    def mixed_sent():
        for group in range(groups):
            block = mixed_ref.at[:, group_lanes(tp, group, 0)]

            @pl.when(jnp.logical_not(keeps(tp, group)))
            def _():
                remote(
                    block, block, swap_send.at[group // 2], swap_recv.at[0, 0], {"lo": 1 - lo}
                ).wait_send()

            for stage in range(len(strides)):
                for which in (0, 1):
                    for mask in range(1 << stage):

                        @pl.when(keeps(origin_of(tp, mask), group))
                        def _():
                            remote(
                                block,
                                block,
                                tp_send.at[(1 << stage) - 1 + mask, which, group // 2],
                                tp_recv.at[0, 0, 0, 0],
                                {"tp": flipped(tp, strides[stage])},
                            ).wait_send()

    early = hi < hi_size // 2
    scope = jax.named_scope

    def local():
        with scope("local"):
            lax.fori_loop(0, heads, local_body, 0)

    def hop_pieces(hop, way, first, last):
        with scope(f"hop{hop}_{way}_{first}"):
            for piece in range(first, last):
                take_hop(hop, way, piece)

    loads[0].wait()
    for piece in range(pieces):
        if piece < 3:
            start_line(0, piece)
        elif piece < 7:

            @pl.when(hi == hi_size - 2)
            def _():
                start_line(0, piece)

        start_line(1, piece)
    for piece in range(pieces):
        start_side(piece)
    loads[1].wait()
    loads[2].wait()
    with scope("state"):
        lax.fori_loop(0, heads, state_body, 0)
    loads[3].wait()
    loads[4].wait()

    @pl.when(jnp.logical_not(early))
    def _():
        local()

    with scope("chain"):
        chain_states()
    for piece in range(3, pieces):
        if piece < 7:

            @pl.when(hi != hi_size - 2)
            def _():
                start_line(0, piece)

        else:
            start_line(0, piece)

    @pl.when(early)
    def _():
        local()

    with scope("take_states"):
        take_states()
    with scope("mix"):
        for span in range(spans):
            mix(span)
            send_away(span)
            if span < 2:
                send_kept(span)
    hop_pieces(1, 1, 0, 6)
    hop_pieces(1, 0, 0, 3)
    with scope("swap01"):
        for span in range(2):
            take_swap(span)
            send_kept(span + 2)
    hop_pieces(1, 1, 6, 8)
    hop_pieces(1, 0, 3, 4)

    def take_rest(span):
        with scope(f"take{span}"):
            for stage in range(1, len(strides)):
                for which in (0, 1):
                    take_stage(stage, which, span)

    with scope("y0"):
        take_stage(0, 0, 0)
        take_swap(2)
        take_stage(0, 0, 1)
        take_stage(0, 1, 0)
    hop_pieces(1, 0, 4, 8)
    hop_pieces(2, 1, 0, 3)
    def near_part(span):
        if hi_size <= 4:
            take_rest(span)
            if span == 0:
                take_near_sides()
            with scope(f"near{span}"):
                multiply_near(span)

    near_part(0)
    with scope("y1"):
        take_swap(3)
        take_stage(0, 0, 2)
        take_stage(0, 1, 1)
        take_stage(0, 0, 3)
    hop_pieces(2, 1, 3, 5)
    hop_pieces(2, 0, 0, 3)
    near_part(1)
    with scope("y2"):
        take_stage(0, 1, 2)
        take_stage(0, 1, 3)
    near_part(2)
    near_part(3)
    hop_pieces(2, 1, 5, 8)
    hop_pieces(2, 0, 3, 8)
    if hi_size > 4:
        for hop in range(3, hi_size - 1):
            for way in (0, 1):
                hop_pieces(hop, way, 0, pieces)
        take_near_sides()
        for span in range(spans):
            take_rest(span)
            multiply_near(span)
    for piece in range(pieces):
        with scope(f"far_wait{piece}"):
            if hi_size > 3:
                for way in (0, 1):
                    take_hop(hi_size - 1, way, piece)
            take_away_sides(piece)
        with scope(f"far{piece}"):
            multiply_away(piece)
        with scope(f"sent{piece}"):
            if piece == 0:
                states_sent()
            if piece == 1:
                mixed_sent()
            if piece == pieces - 3:
                lines_sent(1, 2)
            if piece == pieces - 2:
                lines_sent(2, min(3, hi_size))
            if piece == pieces - 1:
                lines_sent(3, hi_size)
        if piece > 0:
            with scope(f"combine{piece - 1}"):
                for span in range(spans):
                    combine(piece - 1, span)
    with scope("combine_last"):
        for span in range(spans):
            combine(pieces - 1, span)
        for span in range(spans):
            total_squares(span)
        for step in range(1, tp_size):
            square_copy(step).start()
    with scope("drain"):
        for piece in range(pieces):
            for reach in range(1, inner_size):
                for block_hi in range(hi_size):
                    side_copy(reach, block_hi, piece).wait_send()
        remote(
            partial_out, partial_in, partial_send.at[0], partial_recv.at[0, 0], {"lo": 1 - lo}
        ).wait_send()
    with scope("finish"):
        finish()
        for step in range(1, tp_size):
            square_copy(step).wait_send()


def layer(sizes, arrays):
    hi_size, inner_size, tp_size, per, tile, weight_tile = sizes
    rows, width = arrays[0].shape
    depth, columns = arrays[7].shape
    heads = width // HEAD_DIM
    groups = heads // per
    spans = rows // SPAN
    members = 2 * inner_size
    own_heads = heads // members
    kept = (groups + 1) // 2
    half_width = heads * tp_size // 2 * HEAD_DIM
    pieces = columns // weight_tile
    vmem = pl.BlockSpec(memory_space=pltpu.VMEM)
    anywhere = pl.BlockSpec(memory_space=pl.ANY)
    item = (HEAD_DIM + TAIL, HEAD_DIM)
    square = (HEAD_DIM, HEAD_DIM)
    bf16, f32 = jnp.bfloat16, jnp.float32
    dma = pltpu.SemaphoreType.DMA
    return pl.pallas_call(
        functools.partial(layer_kernel, sizes),
        in_specs=[anywhere] * 4 + [vmem] * 3 + [anywhere],
        out_specs=[vmem, vmem],
        out_shape=[
            pltpu.VMEM((rows, columns), bf16),
            pltpu.VMEM((spans, HEAD_DIM), f32),
        ],
        scratch_shapes=[
            pltpu.VMEM((hi_size * inner_size * depth, columns), bf16),
            pltpu.VMEM((rows, width), bf16),
            pltpu.VMEM((rows, width), bf16),
            pltpu.VMEM((rows, width), bf16),
            pltpu.VMEM((rows, width), bf16),
            pltpu.VMEM((rows, width), f32),
            pltpu.VMEM((rows, width), f32),
            pltpu.VMEM((heads, max(8, spans), HEAD_DIM), f32),
            pltpu.VMEM((heads, max(1, spans - 1)) + square, bf16),
            pltpu.VMEM((heads,) + item, bf16),
            pltpu.VMEM((members, own_heads) + item, bf16),
            pltpu.VMEM((own_heads,) + square, bf16),
            pltpu.VMEM((own_heads,) + square, bf16),
            pltpu.VMEM((heads,) + square, bf16),
            pltpu.VMEM((heads,) + square, bf16),
            pltpu.VMEM((rows, width), f32),
            pltpu.VMEM((rows, width), bf16),
            pltpu.VMEM((rows, width), f32),
            pltpu.VMEM((rows, 2 * half_width + width), bf16),
            pltpu.VMEM((pieces, spans, SPAN, weight_tile), bf16),
            pltpu.VMEM((pieces, spans, SPAN, weight_tile), bf16),
            pltpu.VMEM((spans, 2 * SPAN, columns), f32),
            pltpu.VMEM((spans, SPAN, HEAD_DIM), f32),
            pltpu.VMEM((tp_size, max(8, spans), HEAD_DIM), f32),
            dma((5,)),
            dma((1,)),
            dma((members, own_heads)),
            dma((1,)),
            dma((own_heads,)),
            dma((1,)),
            dma((heads,)),
            dma((kept,)),
            dma((kept, spans)),
            dma((tp_size - 1, 2, kept)),
            dma((tp_size - 1, 2, kept, spans)),
            dma((2, max(1, hi_size - 1))),
            dma((hi_size, pieces)),
            dma((2, inner_size - 1, hi_size, pieces) if inner_size > 1 else (1,)),
            dma((1,)),
            dma((pieces, spans)),
            dma((tp_size - 1,)),
            dma((tp_size - 1,)),
        ],
        name="layer",
        compiler_params=pltpu.CompilerParams(
            collective_id=0, has_side_effects=True, vmem_limit_bytes=62800 * 1024
        ),
        cost_estimate=pl.CostEstimate(
            flops=rows * width * 10000, bytes_accessed=14 * rows * width, transcendentals=0
        ),
    )(*arrays)


def per_device(hi_size, inner_size, tp_size, *arrays):
    query, forget, value, gate, gap, surge, head_gain, matrix, branch_gain, residual = arrays
    per = inner_size * matrix.shape[0] // HEAD_DIM
    projected, scale = layer(
        (hi_size, inner_size, tp_size, per, 256, 128),
        (
            query,
            forget,
            value,
            gate,
            gap.reshape(-1, HEAD_DIM),
            surge,
            head_gain.reshape(1, HEAD_DIM),
            matrix,
        ),
    )
    columns = matrix.shape[1]
    gain_part = lax.dynamic_slice_in_dim(branch_gain, lax.axis_index("tp") * columns, columns)
    branch = projected.astype(jnp.float32) * scale.reshape(-1)[:, None] * gain_part
    return (residual.astype(jnp.float32) + branch).astype(jnp.bfloat16)


def solution(mesh):
    sp_size, tp_size = mesh.shape["sp"], mesh.shape["tp"]
    sp = ("hi", "lo", "inner")
    placed = (
        P(sp, "tp"),
        P(sp, "tp"),
        P(sp, "tp"),
        P(sp, "tp"),
        P(),
        P("tp", sp),
        P(),
        P(sp, "tp"),
        P(),
        P(sp, "tp"),
    )

    def whole(*arrays):
        inner = max(1, HEAD_DIM * sp_size // arrays[7].shape[0])
        hi = sp_size // (2 * inner)
        devices = mesh.devices.reshape(hi, 2, inner, tp_size)
        paired = Mesh(devices, ("hi", "lo", "inner", "tp"))
        return jax.shard_map(
            functools.partial(per_device, hi, inner, tp_size),
            mesh=paired,
            in_specs=placed,
            out_specs=P(sp, "tp"),
            check_vma=False,
        )(*arrays)

    return whole
```

profile of v0, /device:TPU:0, one launch (start us, length us, event | category | flops | bytes accessed | tf_op | source)
XLA Modules:
  0.0 85.1 jit_solution(7796739538727331157)
XLA Ops:
  0.0 0.0 copy-start
  0.0 0.0 dynamic-slice-start
  0.0 83.6 %layer.1 = (bf16[512,1024]{1,0:T(8,128)(2,1)S(1)}, f32[4,128]{1,0:T(4,128)S(1)}) custom-call(bf16[512,1024]{1,0:T(8,128)(2,1)} %query_in.1, bf16[512,1024]{1,0:T(8,128)(2,1)} %forget_in.1, bf16[512,1024]{1,0:T(8,128)(2,1)} %value_in.1, bf16[512,1024]{1,0:T(8,128)(2,1)} %gate_in.1, f32[32,128]{1,0:T(8,128)} %bitcast.4, f32[8,512]{1,0:T(8,128)} %surge_ref.1, ...), custom_call_target="tpu_custom_call" | custom-call | flops 5242880000 | bytes 7340032 | tf_op jit(solution)/shard_map/layer/pallas_call | solution.py:835
  83.6 0.0 copy-done
  83.6 0.0 dynamic-slice-done
  83.7 1.4 %add_convert_fusion = bf16[512,1024]{1,0:T(8,128)(2,1)} fusion(bf16[512,1024]{1,0:T(8,128)(2,1)S(1)} %get-tuple-element.7, bf16[512,1024]{1,0:T(8,128)(2,1)S(1)} %copy-done, f32[1024]{0:T(1024)S(1)} %dynamic-slice-done, f32[512]{0:T(512)S(1)} %bitcast.3), kind=kLoop, calls=%fused_computation | loop fusion | flops 3145728 | bytes 3151872 | tf_op jit(solution)/shard_map/convert_element_type | solution.py:916
Async XLA Ops:
  0.0 83.6 %copy-start = (bf16[512,1024]{1,0:T(8,128)(2,1)S(1)}, bf16[512,1024]{1,0:T(8,128)(2,1)}, u32[]{:S(2)}) copy-start(bf16[512,1024]{1,0:T(8,128)(2,1)} %param.19) | copy-start | bytes 3145732
  0.0 83.6 %dynamic-slice-start = ((f32[4096]{0:T(1024)}, s32[]{:T(128)}), f32[1024]{0:T(1024)S(1)}, s32[]{:S(2)}) async-start(f32[4096]{0:T(1024)} %param.18, s32[]{:T(128)} %select_n.3), calls=%async_computation | async-start | bytes 8704 | tf_op jit(solution)/shard_map/dynamic_slice | solution.py:914
where the time goes:
time: 85.8 us; the launch traced here: 85.1 us
  Pallas kernels  83.6 us (97%)
  other arithmetic  1.42 us (2%)
    pallas_call x1, Pallas kernels, layer(): pl.pallas_call(functools.partial(layer_kernel, sizes), in_specs=[anywhere...  83.6 us

commit v1 on v0

--- a/solution.py
+++ b/solution.py
@@ -64,6 +64,7 @@
     projected_ref,
     scale_ref,
     whole_weight,
+    relay,
     query_ref,
     forget_ref,
     value_ref,
@@ -100,7 +101,8 @@
     tp_recv,
     line_send,
     line_recv,
-    side_sems,
+    side_send,
+    side_recv,
     partial_send,
     partial_recv,
     square_send,
@@ -113,14 +115,14 @@
     spans = rows // SPAN
     groups = heads // per
     half_width = heads * tp_size // 2 * HEAD_DIM
-    members = 2 * inner_size
+    members = inner_size
+    lines = 2 * hi_size
     own_heads = heads // members
     tiles = columns // tile
     pieces = columns // weight_tile
-    near = hi_size // 2 * per * HEAD_DIM
-    away = half_width - near
     hi, lo, inner, tp = (lax.axis_index(a) for a in ("hi", "lo", "inner", "tp"))
-    member = lo * inner_size + inner
+    member = inner
+    line = hi * 2 + lo
     strides = []
     by = tp_size // 2
     while by >= 1:
@@ -128,7 +130,10 @@
         by //= 2
 
     def member_at(index):
-        return {"lo": index // inner_size, "inner": index % inner_size}
+        return {"inner": index}
+
+    def on_line(index):
+        return {"hi": index // 2, "lo": index % 2}
 
     def flipped(index, by):
         return index + by - 2 * by * ((index // by) % 2)
@@ -182,60 +187,78 @@
             barrier, inc=1, device_id={"tp": (tp + step) % tp_size}, device_id_type=MESH_ID
         )
     for step in (1, -1):
-        there = hi + step
-        inside = (there >= 0) & (there < hi_size)
+        there = line + step
+        inside = (there >= 0) & (there < lines)
 
         @pl.when(inside)
         def _():
-            pl.semaphore_signal(barrier, inc=1, device_id={"hi": there}, device_id_type=MESH_ID)
+            pl.semaphore_signal(barrier, inc=1, device_id=on_line(there), device_id_type=MESH_ID)
 
         peers = peers + jnp.where(inside, 1, 0)
     pl.semaphore_wait(barrier, peers)
 
+    def piece_lanes(piece):
+        return pl.ds(piece * weight_tile, weight_tile)
+
     def weight_block(block_hi, block_inner, piece):
-        return whole_weight.at[
-            slot_rows(block_hi, block_inner), pl.ds(piece * weight_tile, weight_tile)
-        ]
+        return whole_weight.at[slot_rows(block_hi, block_inner), piece_lanes(piece)]
 
     def step_of(way):
         return 1 if way == 0 else -1
 
+    def line_block(origin, distance, piece):
+        block_hi = origin // 2
+        if distance % 2 == 0:
+            return weight_block(block_hi, inner, piece)
+        return relay.at[
+            pl.ds(pl.multiple_of(block_hi * depth, depth), depth), piece_lanes(piece)
+        ]
+
     def line_copy(way, hop, piece):
-        block = weight_block(hi - step_of(way) * (hop - 1), inner, piece)
+        origin = line - step_of(way) * (hop - 1)
+        return remote(
+            line_block(origin, hop - 1, piece),
+            line_block(origin, hop, piece),
+            line_send.at[way, hop - 1],
+            line_recv.at[origin, piece],
+            on_line(line + step_of(way)),
+        )
+
+    def line_arrival(origin, piece):
+        block = weight_block(hi, inner, piece)
+        return remote(
+            block, block, line_send.at[0, 0], line_recv.at[origin, piece], on_line(origin)
+        )
+
+    def line_sent(way, hop):
+        block = whole_weight.at[slot_rows(hi, inner)]
         return remote(
             block,
             block,
             line_send.at[way, hop - 1],
-            line_recv.at[hi - step_of(way) * (hop - 1), piece],
-            {"hi": hi + step_of(way)},
-        )
-
-    def line_arrival(origin, piece):
-        block = weight_block(origin, inner, piece)
-        return remote(block, block, line_send.at[0, 0], line_recv.at[origin, piece], {"hi": origin})
-
-    def line_sent(way, hop):
-        block = whole_weight.at[slot_rows(0, 0)]
-        return remote(
-            block, block, line_send.at[way, hop - 1], line_recv.at[0, 0], {"hi": hi + step_of(way)}
-        )
+            line_recv.at[0, 0],
+            on_line(line + step_of(way)),
+        )
+
+    def inside(index):
+        return (index >= 0) & (index < lines)
 
     def sends(way, hop):
-        origin = hi - step_of(way) * (hop - 1)
-        target = hi + step_of(way)
-        return (origin >= 0) & (origin < hi_size) & (target >= 0) & (target < hi_size)
+        step = step_of(way)
+        last = line + step * (1 + hop % 2)
+        return inside(line - step * (hop - 1)) & inside(last)
 
     def receives(way, hop):
-        origin = hi - step_of(way) * hop
-        return (origin >= 0) & (origin < hi_size)
+        step = step_of(way)
+        return inside(line - step * hop) & inside(line + step * (hop % 2))
 
     def side_copy(reach, block_hi, piece):
         block = weight_block(block_hi, inner, piece)
         return remote(
             block,
             block,
-            side_sems.at[0, reach - 1, block_hi, piece],
-            side_sems.at[1, reach - 1, block_hi, piece],
+            side_send.at[reach - 1],
+            side_recv.at[reach - 1, block_hi, piece],
             {"inner": (inner + reach) % inner_size},
         )
 
@@ -249,36 +272,37 @@
             side_copy(reach, hi, piece).start()
 
     def take_hop(hop, way, piece):
-        if hop >= hi_size:
+        if hop >= lines:
             return
+        origin = line - step_of(way) * hop
 
         @pl.when(receives(way, hop))
         def _():
-            line_arrival(hi - step_of(way) * hop, piece).wait_recv()
-            for reach in range(1, inner_size):
-                side_copy(reach, hi - step_of(way) * hop, piece).start()
-
-        if hop + 1 < hi_size:
+            line_arrival(origin, piece).wait_recv()
+            if hop % 2 == 0:
+                for reach in range(1, inner_size):
+                    side_copy(reach, origin // 2, piece).start()
+
+        if hop + 1 < lines:
 
             @pl.when(sends(way, hop + 1))
             def _():
                 line_copy(way, hop + 1, piece).start()
 
-    near_first = hi < hi_size // 2
-    near_block = jnp.where(near_first, 0, hi_size - hi_size // 2)
-    away_block = jnp.where(near_first, hi_size // 2, 0)
-    block_depth = per * HEAD_DIM
-
-    def take_near_sides():
+    def take_sides(piece):
         for reach in range(1, inner_size):
-            for number in range(hi_size // 2):
-                for piece in range(pieces):
-                    side_copy(reach, near_block + number, piece).wait_recv()
-
-    def take_away_sides(piece):
+            for block_hi in range(hi_size):
+                side_copy(reach, block_hi, piece).wait_recv()
+
+    def sides_sent():
         for reach in range(1, inner_size):
-            for number in range(hi_size - hi_size // 2):
-                side_copy(reach, away_block + number, piece).wait_recv()
+            remote(
+                whole_weight.at[pl.ds(0, hi_size * depth)],
+                whole_weight.at[pl.ds(0, hi_size * depth)],
+                side_send.at[reach - 1],
+                side_recv.at[0, 0, 0],
+                {"inner": (inner + reach) % inner_size},
+            ).wait_send()
 
     def state_copy(head):
         return remote(
@@ -304,7 +328,7 @@
             chain_in.at[number],
             chain_send.at[0],
             chain_recv.at[number],
-            {"hi": hi + 1},
+            on_line(line + 1),
         )
 
     def deliver_copy(index, number):
@@ -368,7 +392,7 @@
         return carry
 
     def chain_states():
-        @pl.when(hi == 0)
+        @pl.when(line == 0)
         def _():
             chain_in[...] = jnp.zeros_like(chain_in)
 
@@ -379,7 +403,7 @@
                 def _():
                     state_arrival(index, number).wait_recv()
 
-            @pl.when(hi > 0)
+            @pl.when(line > 0)
             def _():
                 chain_copy(number).wait_recv()
 
@@ -391,7 +415,7 @@
                 state = state * (tail[0:1, :] + tail[1:2, :]) + item
             chain_out[number] = state.astype(jnp.bfloat16)
 
-            @pl.when(hi + 1 < hi_size)
+            @pl.when(line + 1 < lines)
             def _():
                 chain_copy(number).start()
 
@@ -536,30 +560,18 @@
 
     def both(span, start, depth):
         part = span_rows(span)
-        start = pl.multiple_of(start, HEAD_DIM)
-        later = pl.multiple_of(start + half_width, HEAD_DIM)
         return jnp.concatenate(
-            [mixed_ref[part, pl.ds(later, depth)], mixed_ref[part, pl.ds(start, depth)]], axis=0
-        )
-
-    def multiply_near(span):
-        start = near_block * block_depth
-        left = both(span, start, near)
-        rows_near = pl.ds(pl.multiple_of(start, HEAD_DIM), near)
-        for number in range(tiles):
-            lanes = pl.ds(number * tile, tile)
-            total_ref[span, :, lanes] = dot(left, whole_weight[rows_near, lanes])
-
-    def multiply_away(piece):
-        start = away_block * block_depth
-        rows_away = pl.ds(pl.multiple_of(start, HEAD_DIM), away)
-        lanes = pl.ds(piece * weight_tile, weight_tile)
-        right = whole_weight[rows_away, lanes]
-        for span in range(spans):
-            total = total_ref[span, :, lanes] + dot(both(span, start, away), right)
+            [mixed_ref[part, half_width : 2 * half_width], mixed_ref[part, 0:half_width]], axis=0
+        )
+
+    def multiply(piece, part):
+        lanes = piece_lanes(piece)
+        right = whole_weight[:, lanes]
+        for span in part:
+            total = dot(both(span, 0, half_width), right)
             partial_out[piece, span] = total[0:SPAN].astype(jnp.bfloat16)
             partial_copy(piece, span).start()
-            total_ref[span, SPAN:, lanes] = total[SPAN:]
+            total_ref[span, :, lanes] = total[SPAN:]
 
     def square_copy(step):
         return remote(
@@ -573,7 +585,7 @@
     def combine(piece, span):
         lanes = pl.ds(piece * weight_tile, weight_tile)
         partial_copy(piece, span).wait_recv()
-        total = total_ref[span, SPAN:, lanes] + partial_in[piece, span].astype(jnp.float32)
+        total = total_ref[span, :, lanes] + partial_in[piece, span].astype(jnp.float32)
         rounded = total.astype(jnp.bfloat16)
         projected_ref[span_rows(span), lanes] = rounded
         branch = rounded.astype(jnp.float32)
@@ -626,10 +638,10 @@
             device_id_type=MESH_ID,
         ).wait_send()
 
-        @pl.when(hi + 1 < hi_size)
+        @pl.when(line + 1 < lines)
         def _():
             remote(
-                chain_out, chain_in, chain_send.at[0], chain_recv.at[0], {"hi": hi + 1}
+                chain_out, chain_in, chain_send.at[0], chain_recv.at[0], on_line(line + 1)
             ).wait_send()
 
     def mixed_sent():
@@ -656,7 +668,9 @@
                                 {"tp": flipped(tp, strides[stage])},
                             ).wait_send()
 
-    early = hi < hi_size // 2
+    early = line < 2
+    ends = (line == 0) | (line == lines - 1)
+    between = jnp.logical_not(ends)
     scope = jax.named_scope
 
     def local():
@@ -668,23 +682,53 @@
             for piece in range(first, last):
                 take_hop(hop, way, piece)
 
+    low = line < lines // 2
+
+    def outward(first, last):
+        @pl.when(low)
+        def _():
+            hop_pieces(1, 1, first, last)
+
+        @pl.when(jnp.logical_not(low))
+        def _():
+            hop_pieces(1, 0, first, last)
+
+    def inward(first, last):
+        @pl.when(low)
+        def _():
+            hop_pieces(1, 0, first, last)
+
+        @pl.when(jnp.logical_not(low))
+        def _():
+            hop_pieces(1, 1, first, last)
+
+    def own_sides(first, last):
+        for piece in range(first, last):
+            start_side(piece)
+
     loads[0].wait()
     for piece in range(pieces):
         if piece < 3:
             start_line(0, piece)
-        elif piece < 7:
-
-            @pl.when(hi == hi_size - 2)
+        elif piece == 3:
+
+            @pl.when(line > 0)
             def _():
                 start_line(0, piece)
 
         start_line(1, piece)
-    for piece in range(pieces):
-        start_side(piece)
+    own_sides(0, 1)
     loads[1].wait()
     loads[2].wait()
     with scope("state"):
         lax.fori_loop(0, heads, state_body, 0)
+    own_sides(1, 3)
+    outward(0, 2)
+
+    @pl.when(jnp.logical_not(low))
+    def _():
+        hop_pieces(1, 1, 0, 2)
+
     loads[3].wait()
     loads[4].wait()
 
@@ -694,20 +738,45 @@
 
     with scope("chain"):
         chain_states()
-    for piece in range(3, pieces):
-        if piece < 7:
-
-            @pl.when(hi != hi_size - 2)
-            def _():
-                start_line(0, piece)
-
-        else:
+
+    @pl.when(line == 0)
+    def _():
+        for piece in range(3, 6):
             start_line(0, piece)
 
+    @pl.when(line > 0)
+    def _():
+        for piece in range(4, pieces):
+            start_line(0, piece)
+
+    @pl.when(between)
+    def _():
+        own_sides(3, pieces)
+
+    outward(2, 4)
+
     @pl.when(early)
     def _():
         local()
 
+    def end_hops(first, last):
+        @pl.when(ends)
+        def _():
+            hop_pieces(2, 1, first, last)
+            hop_pieces(2, 0, first, last)
+
+    def between_hops(first, last):
+        @pl.when(between)
+        def _():
+            hop_pieces(2, 1, first, last)
+            hop_pieces(2, 0, first, last)
+
+
+    @pl.when(low)
+    def _():
+        hop_pieces(1, 0, 0, 2)
+
+    inward(2, 4)
     with scope("take_states"):
         take_states()
     with scope("mix"):
@@ -716,14 +785,36 @@
             send_away(span)
             if span < 2:
                 send_kept(span)
-    hop_pieces(1, 1, 0, 6)
-    hop_pieces(1, 0, 0, 3)
+
+
+    @pl.when(line == 0)
+    def _():
+        for piece in range(6, pieces):
+            start_line(0, piece)
+
+    @pl.when(ends)
+    def _():
+        own_sides(3, 5)
+
+    end_hops(0, 2)
     with scope("swap01"):
         for span in range(2):
             take_swap(span)
             send_kept(span + 2)
-    hop_pieces(1, 1, 6, 8)
-    hop_pieces(1, 0, 3, 4)
+
+    @pl.when(ends)
+    def _():
+        own_sides(5, pieces)
+
+    @pl.when(jnp.logical_not(low))
+    def _():
+        hop_pieces(1, 1, 4, pieces)
+
+    between_hops(0, 2)
+
+    @pl.when(low)
+    def _():
+        hop_pieces(1, 0, 4, 6)
 
     def take_rest(span):
         with scope(f"take{span}"):
@@ -733,78 +824,86 @@
 
     with scope("y0"):
         take_stage(0, 0, 0)
+        take_stage(0, 0, 1)
         take_swap(2)
-        take_stage(0, 0, 1)
+        take_swap(3)
+    outward(4, 6)
+    with scope("y1"):
         take_stage(0, 1, 0)
-    hop_pieces(1, 0, 4, 8)
-    hop_pieces(2, 1, 0, 3)
-    def near_part(span):
-        if hi_size <= 4:
-            take_rest(span)
-            if span == 0:
-                take_near_sides()
-            with scope(f"near{span}"):
-                multiply_near(span)
-
-    near_part(0)
-    with scope("y1"):
-        take_swap(3)
+        take_stage(0, 1, 1)
+    take_rest(0)
+    take_rest(1)
+    outward(6, pieces)
+
+    @pl.when(low)
+    def _():
+        hop_pieces(1, 0, 6, pieces)
+
+    end_hops(2, 4)
+    if lines > 4:
+        between_hops(2, pieces)
+        end_hops(4, pieces)
+    for hop in range(3, lines):
+        for way in (0, 1):
+            hop_pieces(hop, way, 0, pieces)
+    done = []
+    order = []
+
+    def advance(part, first, last):
+        for piece in range(first, last):
+            if not any(piece == other for other, _ in order):
+                with scope(f"sides{piece}"):
+                    take_sides(piece)
+            with scope(f"mult{part[0]}_{piece}"):
+                multiply(piece, part)
+            order.append((piece, part))
+            if len(order) - len(done) > 4:
+                settle()
+
+    def settle():
+        piece, part = order[len(done)]
+        done.append(piece)
+        with scope(f"comb{part[0]}_{piece}"):
+            for span in part:
+                combine(piece, span)
+
+    half_a, half_b = (0, 1), (2, 3)
+    advance(half_a, 0, 2)
+    with scope("y2"):
         take_stage(0, 0, 2)
-        take_stage(0, 1, 1)
         take_stage(0, 0, 3)
-    hop_pieces(2, 1, 3, 5)
-    hop_pieces(2, 0, 0, 3)
-    near_part(1)
-    with scope("y2"):
+    if lines <= 4:
+        between_hops(2, 4)
+    advance(half_a, 2, 4)
+    with scope("y3"):
         take_stage(0, 1, 2)
         take_stage(0, 1, 3)
-    near_part(2)
-    near_part(3)
-    hop_pieces(2, 1, 5, 8)
-    hop_pieces(2, 0, 3, 8)
-    if hi_size > 4:
-        for hop in range(3, hi_size - 1):
-            for way in (0, 1):
-                hop_pieces(hop, way, 0, pieces)
-        take_near_sides()
-        for span in range(spans):
-            take_rest(span)
-            multiply_near(span)
-    for piece in range(pieces):
-        with scope(f"far_wait{piece}"):
-            if hi_size > 3:
-                for way in (0, 1):
-                    take_hop(hi_size - 1, way, piece)
-            take_away_sides(piece)
-        with scope(f"far{piece}"):
-            multiply_away(piece)
-        with scope(f"sent{piece}"):
-            if piece == 0:
-                states_sent()
-            if piece == 1:
-                mixed_sent()
-            if piece == pieces - 3:
-                lines_sent(1, 2)
-            if piece == pieces - 2:
-                lines_sent(2, min(3, hi_size))
-            if piece == pieces - 1:
-                lines_sent(3, hi_size)
-        if piece > 0:
-            with scope(f"combine{piece - 1}"):
-                for span in range(spans):
-                    combine(piece - 1, span)
+    take_rest(2)
+    take_rest(3)
+    if lines <= 4:
+        end_hops(4, 6)
+        between_hops(4, 6)
+    advance(half_b, 0, 4)
+    if lines <= 4:
+        between_hops(6, pieces)
+        end_hops(6, pieces)
+    states_sent()
+    mixed_sent()
+    advance(half_a, 4, 6)
+    advance(half_b, 4, 6)
+    lines_sent(1, lines)
+    advance(half_a, 6, pieces)
+    advance(half_b, 6, pieces)
+    sides_sent()
+    while len(order) - len(done) > 1:
+        settle()
     with scope("combine_last"):
-        for span in range(spans):
-            combine(pieces - 1, span)
+        settle()
         for span in range(spans):
             total_squares(span)
         for step in range(1, tp_size):
             square_copy(step).start()
     with scope("drain"):
-        for piece in range(pieces):
-            for reach in range(1, inner_size):
-                for block_hi in range(hi_size):
-                    side_copy(reach, block_hi, piece).wait_send()
         remote(
             partial_out, partial_in, partial_send.at[0], partial_recv.at[0, 0], {"lo": 1 - lo}
         ).wait_send()
@@ -821,7 +920,7 @@
     heads = width // HEAD_DIM
     groups = heads // per
     spans = rows // SPAN
-    members = 2 * inner_size
+    members = inner_size
     own_heads = heads // members
     kept = (groups + 1) // 2
     half_width = heads * tp_size // 2 * HEAD_DIM
@@ -842,6 +941,7 @@
         ],
         scratch_shapes=[
             pltpu.VMEM((hi_size * inner_size * depth, columns), bf16),
+            pltpu.VMEM((hi_size * depth, columns), bf16),
             pltpu.VMEM((rows, width), bf16),
             pltpu.VMEM((rows, width), bf16),
             pltpu.VMEM((rows, width), bf16),
@@ -862,7 +962,7 @@
             pltpu.VMEM((rows, 2 * half_width + width), bf16),
             pltpu.VMEM((pieces, spans, SPAN, weight_tile), bf16),
             pltpu.VMEM((pieces, spans, SPAN, weight_tile), bf16),
-            pltpu.VMEM((spans, 2 * SPAN, columns), f32),
+            pltpu.VMEM((spans, SPAN, columns), f32),
             pltpu.VMEM((spans, SPAN, HEAD_DIM), f32),
             pltpu.VMEM((tp_size, max(8, spans), HEAD_DIM), f32),
             dma((5,)),
@@ -876,9 +976,10 @@
             dma((kept, spans)),
             dma((tp_size - 1, 2, kept)),
             dma((tp_size - 1, 2, kept, spans)),
-            dma((2, max(1, hi_size - 1))),
-            dma((hi_size, pieces)),
-            dma((2, inner_size - 1, hi_size, pieces) if inner_size > 1 else (1,)),
+            dma((2, 2 * hi_size - 1)),
+            dma((2 * hi_size, pieces)),
+            dma((inner_size - 1,)),
+            dma((inner_size - 1, hi_size, pieces)),
             dma((1,)),
             dma((pieces, spans)),
             dma((tp_size - 1,)),
@@ -933,7 +1034,7 @@
     )
 
     def whole(*arrays):
-        inner = max(1, HEAD_DIM * sp_size // arrays[7].shape[0])
+        inner = max(2, HEAD_DIM * sp_size // arrays[7].shape[0])
         hi = sp_size // (2 * inner)
         devices = mesh.devices.reshape(hi, 2, inner, tp_size)
         paired = Mesh(devices, ("hi", "lo", "inner", "tp"))

time: 85.8 us -> 78.9 us (0.920)
  Pallas kernels: 83.6 us -> 76.9 us
    pallas_call x1, Pallas kernels: 83.6 us -> 76.9 us  [layer(): pl.pallas_call(functools.partial(layer_kernel, sizes), in_specs=[anywhere...]
where the time goes in v1:
time: 78.9 us; the launch traced here: 78.4 us
  Pallas kernels  76.9 us (97%)
  other arithmetic  1.42 us (2%)
    pallas_call x1, Pallas kernels, layer(): pl.pallas_call(functools.partial(layer_kernel, sizes), in_specs=[anywhere...  76.9 us

profile of v1, /device:TPU:0, one launch (start us, length us, event | category | flops | bytes accessed | tf_op | source)
XLA Modules:
  0.0 78.4 jit_solution(13524495971301109688)
XLA Ops:
  0.0 0.0 copy-start
  0.0 0.0 dynamic-slice-start
  0.0 76.9 %layer.1 = (bf16[512,1024]{1,0:T(8,128)(2,1)S(1)}, f32[4,128]{1,0:T(4,128)S(1)}) custom-call(bf16[512,1024]{1,0:T(8,128)(2,1)} %query_in.1, bf16[512,1024]{1,0:T(8,128)(2,1)} %forget_in.1, bf16[512,1024]{1,0:T(8,128)(2,1)} %value_in.1, bf16[512,1024]{1,0:T(8,128)(2,1)} %gate_in.1, f32[32,128]{1,0:T(8,128)} %bitcast.4, f32[8,512]{1,0:T(8,128)} %surge_ref.1, ...), custom_call_target="tpu_custom_call" | custom-call | flops 5242880000 | bytes 7340032 | tf_op jit(solution)/shard_map/layer/pallas_call | solution.py:934
  76.9 0.0 copy-done
  76.9 0.0 dynamic-slice-done
  77.0 1.4 %add_convert_fusion = bf16[512,1024]{1,0:T(8,128)(2,1)} fusion(bf16[512,1024]{1,0:T(8,128)(2,1)S(1)} %get-tuple-element.7, bf16[512,1024]{1,0:T(8,128)(2,1)S(1)} %copy-done, f32[1024]{0:T(1024)S(1)} %dynamic-slice-done, f32[512]{0:T(512)S(1)} %bitcast.3), kind=kLoop, calls=%fused_computation | loop fusion | flops 3145728 | bytes 3151872 | tf_op jit(solution)/shard_map/convert_element_type | solution.py:1017
Async XLA Ops:
  0.0 76.9 %copy-start = (bf16[512,1024]{1,0:T(8,128)(2,1)S(1)}, bf16[512,1024]{1,0:T(8,128)(2,1)}, u32[]{:S(2)}) copy-start(bf16[512,1024]{1,0:T(8,128)(2,1)} %param.19) | copy-start | bytes 3145732
  0.0 76.9 %dynamic-slice-start = ((f32[4096]{0:T(1024)}, s32[]{:T(128)}), f32[1024]{0:T(1024)S(1)}, s32[]{:S(2)}) async-start(f32[4096]{0:T(1024)} %param.18, s32[]{:T(128)} %select_n.3), calls=%async_computation | async-start | bytes 8704 | tf_op jit(solution)/shard_map/dynamic_slice | solution.py:1015

commit v2 on v1

--- a/solution.py
+++ b/solution.py
@@ -350,8 +350,7 @@
             member_at(head // own_heads),
         )
 
-    def state_body(turn, carry):
-        head = (turn + (member + 1) * own_heads) % heads
+    def head_state(head):
         causal = lower_triangle()
         gap = gap_ref[pl.ds(tp * heads + head, 1), :]
         lanes = lanes_of(head)
@@ -378,16 +377,21 @@
         tail = jnp.where(first, high, decay - high).astype(jnp.bfloat16)
         state_out[head, 0:HEAD_DIM, :] = item
         state_out[head, HEAD_DIM:, :] = tail
-        owner = head // own_heads
-
-        @pl.when(owner == member)
-        def _():
-            gathered[member, head % own_heads, 0:HEAD_DIM, :] = item
-            gathered[member, head % own_heads, HEAD_DIM:, :] = tail
-
-        @pl.when(owner != member)
-        def _():
-            state_copy(head).start()
+
+    def state_body(turn, carry):
+        pair = [(turn * 2 + number + (member + 1) * own_heads) % heads for number in range(2)]
+        for head in pair:
+            head_state(head)
+        for head in pair:
+            owner = head // own_heads
+
+            @pl.when(owner == member)
+            def _():
+                gathered[member, head % own_heads] = state_out[head]
+
+            @pl.when(owner != member)
+            def _():
+                state_copy(head).start()
 
         return carry
 
@@ -644,7 +648,7 @@
                 chain_out, chain_in, chain_send.at[0], chain_recv.at[0], on_line(line + 1)
             ).wait_send()
 
-    def mixed_sent():
+    def swaps_sent():
         for group in range(groups):
             block = mixed_ref.at[:, group_lanes(tp, group, 0)]
 
@@ -653,6 +657,10 @@
                 remote(
                     block, block, swap_send.at[group // 2], swap_recv.at[0, 0], {"lo": 1 - lo}
                 ).wait_send()
+
+    def mixed_sent():
+        for group in range(groups):
+            block = mixed_ref.at[:, group_lanes(tp, group, 0)]
 
             for stage in range(len(strides)):
                 for which in (0, 1):
@@ -721,7 +729,7 @@
     loads[1].wait()
     loads[2].wait()
     with scope("state"):
-        lax.fori_loop(0, heads, state_body, 0)
+        lax.fori_loop(0, heads // 2, state_body, 0)
     own_sides(1, 3)
     outward(0, 2)
 
@@ -748,6 +756,10 @@
     def _():
         for piece in range(4, pieces):
             start_line(0, piece)
+
+    @pl.when(ends)
+    def _():
+        own_sides(3, 6)
 
     @pl.when(between)
     def _():
@@ -787,30 +799,37 @@
                 send_kept(span)
 
 
-    @pl.when(line == 0)
-    def _():
-        for piece in range(6, pieces):
-            start_line(0, piece)
-
-    @pl.when(ends)
-    def _():
-        own_sides(3, 5)
-
-    end_hops(0, 2)
+    end_hops(0, 4)
+    keeper = keeps(tp, 0)
+
+    @pl.when(jnp.logical_not(keeper))
+    def _():
+        between_hops(0, 2)
+
     with scope("swap01"):
         for span in range(2):
             take_swap(span)
             send_kept(span + 2)
 
-    @pl.when(ends)
-    def _():
-        own_sides(5, pieces)
+    with scope("swapsent"):
+        swaps_sent()
+
+    @pl.when(line == 0)
+    def _():
+        for piece in range(6, pieces):
+            start_line(0, piece)
+
+    outward(4, 6)
 
     @pl.when(jnp.logical_not(low))
     def _():
         hop_pieces(1, 1, 4, pieces)
 
-    between_hops(0, 2)
+
+    @pl.when(keeper)
+    def _():
+        between_hops(0, 2)
+
 
     @pl.when(low)
     def _():
@@ -827,19 +846,23 @@
         take_stage(0, 0, 1)
         take_swap(2)
         take_swap(3)
-    outward(4, 6)
+    outward(6, pieces)
+
+    @pl.when(ends)
+    def _():
+        own_sides(6, pieces)
+
+    if lines <= 4:
+        between_hops(2, 4)
     with scope("y1"):
         take_stage(0, 1, 0)
         take_stage(0, 1, 1)
     take_rest(0)
     take_rest(1)
-    outward(6, pieces)
-
     @pl.when(low)
     def _():
         hop_pieces(1, 0, 6, pieces)
 
-    end_hops(2, 4)
     if lines > 4:
         between_hops(2, pieces)
         end_hops(4, pieces)
@@ -873,7 +896,8 @@
         take_stage(0, 0, 2)
         take_stage(0, 0, 3)
     if lines <= 4:
-        between_hops(2, 4)
+        end_hops(4, 6)
+        between_hops(4, 6)
     advance(half_a, 2, 4)
     with scope("y3"):
         take_stage(0, 1, 2)
@@ -881,12 +905,9 @@
     take_rest(2)
     take_rest(3)
     if lines <= 4:
-        end_hops(4, 6)
-        between_hops(4, 6)
-    advance(half_b, 0, 4)
-    if lines <= 4:
         between_hops(6, pieces)
         end_hops(6, pieces)
+    advance(half_b, 0, 4)
     states_sent()
     mixed_sent()
     advance(half_a, 4, 6)

time: 78.9 us -> 77.5 us (0.982)
  Pallas kernels: 76.9 us -> 75.9 us
    pallas_call x1, Pallas kernels: 76.9 us -> 75.9 us  [layer(): pl.pallas_call(functools.partial(layer_kernel, sizes), in_specs=[anywhere...]
where the time goes in v2:
time: 77.5 us; the launch traced here: 77.3 us
  Pallas kernels  75.9 us (98%)
  other arithmetic  1.42 us (2%)
    pallas_call x1, Pallas kernels, layer(): pl.pallas_call(functools.partial(layer_kernel, sizes), in_specs=[anywhere...  75.9 us

profile of v2, /device:TPU:0, one launch (start us, length us, event | category | flops | bytes accessed | tf_op | source)
XLA Modules:
  0.0 77.3 jit_solution(6601483601071076597)
XLA Ops:
  0.0 0.0 copy-start
  0.0 0.0 dynamic-slice-start
  0.0 75.9 %layer.1 = (bf16[512,1024]{1,0:T(8,128)(2,1)S(1)}, f32[4,128]{1,0:T(4,128)S(1)}) custom-call(bf16[512,1024]{1,0:T(8,128)(2,1)} %query_in.1, bf16[512,1024]{1,0:T(8,128)(2,1)} %forget_in.1, bf16[512,1024]{1,0:T(8,128)(2,1)} %value_in.1, bf16[512,1024]{1,0:T(8,128)(2,1)} %gate_in.1, f32[32,128]{1,0:T(8,128)} %bitcast.4, f32[8,512]{1,0:T(8,128)} %surge_ref.1, ...), custom_call_target="tpu_custom_call" | custom-call | flops 5242880000 | bytes 7340032 | tf_op jit(solution)/shard_map/layer/pallas_call | solution.py:955
  75.9 0.0 copy-done
  75.9 0.0 dynamic-slice-done
  75.9 1.4 %add_convert_fusion = bf16[512,1024]{1,0:T(8,128)(2,1)} fusion(bf16[512,1024]{1,0:T(8,128)(2,1)S(1)} %get-tuple-element.7, bf16[512,1024]{1,0:T(8,128)(2,1)S(1)} %copy-done, f32[1024]{0:T(1024)S(1)} %dynamic-slice-done, f32[512]{0:T(512)S(1)} %bitcast.3), kind=kLoop, calls=%fused_computation | loop fusion | flops 3145728 | bytes 3151872 | tf_op jit(solution)/shard_map/convert_element_type | solution.py:1038
Async XLA Ops:
  0.0 75.9 %copy-start = (bf16[512,1024]{1,0:T(8,128)(2,1)S(1)}, bf16[512,1024]{1,0:T(8,128)(2,1)}, u32[]{:S(2)}) copy-start(bf16[512,1024]{1,0:T(8,128)(2,1)} %param.19) | copy-start | bytes 3145732
  0.0 75.9 %dynamic-slice-start = ((f32[4096]{0:T(1024)}, s32[]{:T(128)}), f32[1024]{0:T(1024)S(1)}, s32[]{:S(2)}) async-start(f32[4096]{0:T(1024)} %param.18, s32[]{:T(128)} %select_n.3), calls=%async_computation | async-start | bytes 8704 | tf_op jit(solution)/shard_map/dynamic_slice | solution.py:1036

commit v3 on v2

--- a/solution.py
+++ b/solution.py
@@ -749,7 +749,7 @@
 
     @pl.when(line == 0)
     def _():
-        for piece in range(3, 6):
+        for piece in range(3, 7):
             start_line(0, piece)
 
     @pl.when(line > 0)
@@ -789,6 +789,7 @@
         hop_pieces(1, 0, 0, 2)
 
     inward(2, 4)
+    outward(4, 5)
     with scope("take_states"):
         take_states()
     with scope("mix"):
@@ -816,10 +817,10 @@
 
     @pl.when(line == 0)
     def _():
-        for piece in range(6, pieces):
+        for piece in range(7, pieces):
             start_line(0, piece)
 
-    outward(4, 6)
+    outward(5, 6)
 
     @pl.when(jnp.logical_not(low))
     def _():

time: 77.5 us -> 77.1 us (level)
  no operation moved by 1% of the time
where the time goes in v3:
time: 77.1 us; the launch traced here: 77 us
  Pallas kernels  75.5 us (98%)
  other arithmetic  1.42 us (2%)
    pallas_call x1, Pallas kernels, layer(): pl.pallas_call(functools.partial(layer_kernel, sizes), in_specs=[anywhere...  75.5 us

profile of v3, /device:TPU:0, one launch (start us, length us, event | category | flops | bytes accessed | tf_op | source)
XLA Modules:
  0.0 77.0 jit_solution(12877814277433977248)
XLA Ops:
  0.0 0.0 copy-start
  0.0 0.0 dynamic-slice-start
  0.0 75.5 %layer.1 = (bf16[512,1024]{1,0:T(8,128)(2,1)S(1)}, f32[4,128]{1,0:T(4,128)S(1)}) custom-call(bf16[512,1024]{1,0:T(8,128)(2,1)} %query_in.1, bf16[512,1024]{1,0:T(8,128)(2,1)} %forget_in.1, bf16[512,1024]{1,0:T(8,128)(2,1)} %value_in.1, bf16[512,1024]{1,0:T(8,128)(2,1)} %gate_in.1, f32[32,128]{1,0:T(8,128)} %bitcast.4, f32[8,512]{1,0:T(8,128)} %surge_ref.1, ...), custom_call_target="tpu_custom_call" | custom-call | flops 5242880000 | bytes 7340032 | tf_op jit(solution)/shard_map/layer/pallas_call | solution.py:956
  75.5 0.0 copy-done
  75.5 0.0 dynamic-slice-done
  75.5 1.4 %add_convert_fusion = bf16[512,1024]{1,0:T(8,128)(2,1)} fusion(bf16[512,1024]{1,0:T(8,128)(2,1)S(1)} %get-tuple-element.7, bf16[512,1024]{1,0:T(8,128)(2,1)S(1)} %copy-done, f32[1024]{0:T(1024)S(1)} %dynamic-slice-done, f32[512]{0:T(512)S(1)} %bitcast.3), kind=kLoop, calls=%fused_computation | loop fusion | flops 3145728 | bytes 3151872 | tf_op jit(solution)/shard_map/convert_element_type | solution.py:1039
Async XLA Ops:
  0.0 75.5 %copy-start = (bf16[512,1024]{1,0:T(8,128)(2,1)S(1)}, bf16[512,1024]{1,0:T(8,128)(2,1)}, u32[]{:S(2)}) copy-start(bf16[512,1024]{1,0:T(8,128)(2,1)} %param.19) | copy-start | bytes 3145732
  0.0 75.5 %dynamic-slice-start = ((f32[4096]{0:T(1024)}, s32[]{:T(128)}), f32[1024]{0:T(1024)S(1)}, s32[]{:S(2)}) async-start(f32[4096]{0:T(1024)} %param.18, s32[]{:T(128)} %select_n.3), calls=%async_computation | async-start | bytes 8704 | tf_op jit(solution)/shard_map/dynamic_slice | solution.py:1037
